TPU v7x, 32 devices: a whole 2x2x4 slice. The times are simulated.
32 devices in a mesh: ep: 8 (over z, core), tp: 4 (over y, x).
Axes of the slice: x: 2, y: 2, z: 4, core: 2. Of those that a mesh axis runs over, the one named last changes fastest.
Arguments:
- tokens: bfloat16 [128, 4096], P('ep', 'tp'), may hold values from -40 to 40
- norm_gain: bfloat16 [4096], P('tp'), may hold values from 0.099609375 to 1.8984375
- routes: int32 [128, 4], P('ep'), may hold values from 0 to 7, all different within a row; in each aligned block of 16 rows (0 to 15, 16 to 31, ...) at most 16 rows name the same one
- route_weights: float32 [128, 4], P('ep'), may hold values from 0.05 to 1
- w_gate: bfloat16 [8, 4096, 4096], P('ep', None, 'tp'), may hold values from -0.25 to 0.25
- w_up: bfloat16 [8, 4096, 4096], P('ep', None, 'tp'), may hold values from -0.25 to 0.25
- w_down: bfloat16 [8, 4096, 4096], P('ep', 'tp'), may hold values from -0.0234375 to 0.0234375
Outputs:
- mixed: bfloat16 [128, 4096], P('ep', 'tp')
Inputs may be any that keep to these rules, and one draw needn't show every extreme that they name: `routes`: within the 16 rows of one device, each token names 4 different experts, and no expert is named by more than 16 rows; some expert reaches 16.
All inputs are finite; a program needn't handle non-finite values.
Results may differ from a plain program's by a relative error of at most 0.018.
Values may be sent and summed in bfloat16 or wider, within the bound.
A program may use at most 64 MiB of HBM per device.

v0:
```python
import jax
import jax.numpy as jnp
from jax import lax
from jax.sharding import PartitionSpec as P


def shards(tokens, norm_gain, routes, route_weights, w_gate, w_up, w_down):
    tok_rows = tokens.shape[0]
    topk = routes.shape[1]
    groups = lax.axis_size("ep")
    capacity = min(tok_rows, max(2, 2 * tok_rows * topk // groups))
    slot_rows = groups * capacity
    flat = routes.reshape(-1)
    order = jnp.arange(flat.shape[0], dtype=jnp.int32)
    earlier = (flat[:, None] == flat[None, :]) & (order[:, None] > order[None, :])
    slot = jnp.sum(earlier.astype(jnp.int32), axis=1)
    target = (flat * capacity + slot).reshape(tok_rows, topk)
    slot_ids = jnp.arange(slot_rows, dtype=jnp.int32)
    picker = jnp.any(target[None, :, :] == slot_ids[:, None, None], axis=2).astype(jnp.bfloat16)
    combine = jnp.sum(
        jnp.where(target[:, :, None] == slot_ids[None, None, :], route_weights[:, :, None], 0.0),
        axis=1,
    )
    whole, gain_whole = (
        lax.all_gather(tokens, "tp", axis=1, tiled=True),
        lax.all_gather(norm_gain.reshape(1, -1), "tp", axis=1, tiled=True),
    )
    full_values = whole.astype(jnp.float32)
    scale = lax.rsqrt(jnp.mean(full_values * full_values, axis=1, keepdims=True) + 1e-05)
    normed = (full_values * scale * gain_whole.astype(jnp.float32)).astype(jnp.bfloat16)
    outbound = jnp.dot(picker, normed, preferred_element_type=jnp.float32).astype(jnp.bfloat16)
    arrived = lax.all_to_all(
        outbound.reshape(groups, capacity, -1), "ep", split_axis=0, concat_axis=0, tiled=True
    ).reshape(slot_rows, -1)
    gate_pre = jnp.dot(arrived, w_gate[0], preferred_element_type=jnp.float32)
    up_pre = jnp.dot(arrived, w_up[0], preferred_element_type=jnp.float32)
    gated = jnp.minimum(gate_pre, 7.0)
    upper = jnp.clip(up_pre, -7.0, 7.0)
    hidden = ((upper + 1.0) * gated * jax.nn.sigmoid(1.702 * gated)).astype(jnp.bfloat16)
    partial_out = jnp.dot(hidden, w_down[0], preferred_element_type=jnp.float32).astype(
        jnp.bfloat16
    )
    summed = (
        lax.psum_scatter(partial_out, "tp", scatter_dimension=1, tiled=True)
        .astype(jnp.float32)
        .astype(jnp.bfloat16)
    )
    returned = lax.all_to_all(
        summed.reshape(groups, capacity, -1), "ep", split_axis=0, concat_axis=0, tiled=True
    ).reshape(slot_rows, -1)
    mixed = jnp.dot(combine, returned.astype(jnp.float32), precision=lax.Precision.HIGHEST)
    return mixed.astype(jnp.bfloat16)


def solution(mesh):
    placed = (
        P("ep", "tp"),
        P("tp"),
        P("ep", None),
        P("ep", None),
        P("ep", None, "tp"),
        P("ep", None, "tp"),
        P("ep", "tp", None),
    )
    return jax.shard_map(
        shards, mesh=mesh, in_specs=placed, out_specs=P("ep", "tp"), check_vma=False
    )
```

profile of v0, /device:TPU:0, one launch (start us, length us, event | category | flops | bytes accessed | tf_op | source)
XLA Modules:
  0.0 120.4 jit_solution(6978321878295605920)
XLA Ops:
  6.5 0.0 reduce-scatter.2.cloned.1.call-start
  6.5 10.1 %all_gather.6 = bf16[16,4096]{1,0:T(8,128)(2,1)S(1)} all-gather(bf16[16,1024]{1,0:T(8,128)(2,1)} %param.7), channel_id=1, replica_groups=mesh['ep'=8,'tp'=4] {'tp'}, dimensions={1}, use_global_device_ids=true | all-gather | bytes 163840 | tf_op jit(solution)/shard_map/all_gather | solution.py:25
  16.7 0.1 fusion.34
  16.8 0.8 copy.21
  17.6 0.1 eq.20
  17.7 0.2 convert_reduce_fusion
  17.9 0.1 reduce_sum.30
  17.9 0.1 copy.22
  18.0 0.7 multiply_add_fusion
  18.7 0.1 fusion.45
  18.8 7.9 %all-gather = bf16[4096]{0:T(1024)(128)(2,1)S(1)} all-gather(bf16[1024]{0:T(1024)(128)(2,1)} %param.8), channel_id=2, replica_groups=mesh['ep'=8,'tp'=4] {'tp'}, dimensions={0}, use_global_device_ids=true | all-gather | bytes 10240 | tf_op jit(solution)/shard_map/all_gather | solution.py:26
  26.7 0.5 convolution_convert_fusion
  27.2 31.2 %all_to_all.10 = bf16[8,16,4096]{2,1,0:T(8,128)(2,1)S(1)} all-to-all(bf16[8,16,4096]{2,1,0:T(8,128)(2,1)S(1)} %bitcast.36), channel_id=1, replica_groups=mesh['ep'=8,'tp'=4] {'ep'}, dimensions={0} | all-to-all | bytes 2097152 | tf_op jit(solution)/shard_map/all_to_all | solution.py:32
  58.4 4.6 %fusion.9 = f32[128,1024]{1,0:T(8,128)S(1)} fusion(bf16[128,4096]{1,0:T(8,128)(2,1)S(1)} %bitcast.34, bf16[1,4096,1024]{2,1,0:T(8,128)(2,1)} %param.11), kind=kOutput, calls=%fused_computation.8 | convolution fusion | flops 1073872896 | bytes 9961472 | tf_op jit(solution)/shard_map/dot_general | solution.py:35
  63.1 0.0 copy-start
  63.1 9.3 %fusion.6 = bf16[128,4096]{1,0:T(8,128)(2,1)} fusion(bf16[1,1024,4096]{2,1,0:T(8,128)(2,1)} %param.13, f32[128,1024]{1,0:T(8,128)S(1)} %fusion.9, bf16[128,4096]{1,0:T(8,128)(2,1)S(1)} %bitcast.35, bf16[1,4096,1024]{2,1,0:T(8,128)(2,1)} %param.12), kind=kOutput, calls=%fused_computation.6 | convolution fusion | flops 2149187584 | bytes 19398656 | tf_op jit(solution)/shard_map/dot_general | solution.py:40
  72.4 0.0 reduce-scatter.2.cloned.1.call-update
  72.4 26.0 %reduce-scatter.2.cloned.1.call-done = bf16[128,1024]{1,0:T(8,128)(2,1)} async-done(((bf16[128,4096]{1,0:T(8,128)(2,1)}), bf16[128,1024]{1,0:T(8,128)(2,1)}) %reduce-scatter.2.cloned.1.call-update) | async-done | bytes 262160 | tf_op jit(solution)/shard_map/reduce_scatter | solution.py:44
  98.4 4.6 %all-to-all-start.1 = ((bf16[8,16,1024]{2,1,0:T(8,128)(2,1)}), bf16[8,16,1024]{2,1,0:T(8,128)(2,1)S(1)}, u32[]{:S(2)}, u32[]{:S(2)}) async-start(bf16[8,16,1024]{2,1,0:T(8,128)(2,1)} %bitcast.38), calls=%async_computation.2 | async-start | bytes 524288 | tf_op jit(solution)/shard_map/all_to_all | solution.py:48
  103.0 0.0 copy-done
  103.1 0.1 select_reduce_fusion
  103.1 9.6 %all-to-all-done.1 = bf16[8,16,1024]{2,1,0:T(8,128)(2,1)S(1)} async-done(((bf16[8,16,1024]{2,1,0:T(8,128)(2,1)}), bf16[8,16,1024]{2,1,0:T(8,128)(2,1)S(1)}, u32[]{:S(2)}, u32[]{:S(2)}) %all-to-all-start.1) | async-done | bytes 262176 | tf_op jit(solution)/shard_map/all_to_all | solution.py:48
  112.8 0.8 convolution_convert_fusion.1
  (2 shorter events, 0.0 us)
Async XLA Ops:
  6.5 91.9 %reduce-scatter.2.cloned.1.call-start = ((), (), s32[]{:S(2)}) async-start(), calls=%async_computation.3 | async-start | bytes 1310720 | tf_op jit(solution)/shard_map/reduce_scatter | solution.py:44
  63.1 40.0 %copy-start = (f32[16,4]{0,1:T(4,128)S(1)}, f32[16,4]{0,1:T(4,128)}, u32[]{:S(2)}) copy-start(f32[16,4]{0,1:T(4,128)} %param.10) | copy-start | bytes 772
  98.4 14.3 %all-to-all-start.1 = ((bf16[8,16,1024]{2,1,0:T(8,128)(2,1)}), bf16[8,16,1024]{2,1,0:T(8,128)(2,1)S(1)}, u32[]{:S(2)}, u32[]{:S(2)}) async-start(bf16[8,16,1024]{2,1,0:T(8,128)(2,1)} %bitcast.38), calls=%async_computation.2 | async-start | bytes 524288 | tf_op jit(solution)/shard_map/all_to_all | solution.py:48
Sparse Core Ops, SparseCore 0:
  72.5 25.8 reduce-scatter.1
where the time goes:
time: 121 us; the launch traced here: 120 us
  blocking collectives  49.2 us (41%)
  waiting for transfers between devices  35.7 us (30%)
  matrix products  15.2 us (13%)
  between operations  13.4 us (11%)
  starting transfers between devices  4.62 us (4%)
    all_to_all x1, blocking collectives, shards(): lax.all_to_all(outbound.reshape(groups, capacity, -1), 'ep', split_axis=0...  31.2 us
    reduce_scatter x1, waiting for transfers between devices, shards(): lax.psum_scatter(partial_out, 'tp', scatter_dimension=1, tiled=True)  26 us
    all_gather x1, blocking collectives, shards(): lax.all_gather(tokens, 'tp', axis=1, tiled=True)  10.1 us
    all_to_all x1, waiting for transfers between devices, shards(): lax.all_to_all(summed.reshape(groups, capacity, -1), 'ep', split_axis=0,...  9.62 us
    dot_general x1, matrix products, shards(): jnp.dot(hidden, w_down[0], preferred_element_type=jnp.float32)  9.29 us
    all_gather x1, blocking collectives, shards(): lax.all_gather(norm_gain.reshape(1, -1), 'tp', axis=1, tiled=True)  7.86 us
    dot_general x1, matrix products, shards(): gate_pre = jnp.dot(arrived, w_gate[0], preferred_element_type=jnp.float32)  4.63 us
    all_to_all x1, starting transfers between devices, shards(): lax.all_to_all(summed.reshape(groups, capacity, -1), 'ep', split_axis=0,...  4.61 us
  transfers between devices with their start and end apart: 2, of which 2 were waited for; matrix products, arithmetic and copies ran while one was open for 0% of the time, Pallas kernels for 0%

commit v1 on v0

v1 whole, which is shorter than its diff:
```python
import functools

import jax
import jax.numpy as jnp
from jax import lax
from jax.experimental import pallas as pl
from jax.experimental.pallas import tpu as pltpu
from jax.sharding import PartitionSpec as P

MESH = pl.DeviceIdType.MESH
CORES = 2
EXTRA = 128
HALF_EXTRA = EXTRA // 2
SQUARES = HALF_EXTRA - 2


def flip(index, bits):
    bit = 1
    while bit <= bits:
        if bits & bit:
            index = index + bit - 2 * bit * ((index // bit) % 2)
        bit *= 2
    return index


def kernel(
    n_z, n_tp,
    tokens, gain, routes, route_weights, w_gate, w_up, w_down,
    out,
    gate_v, up_v, down_v, gathered, acc_gate, acc_up, hidden,
    pair_send, pair_recv, pair_own, tp_send, tp_recv, z_send, z_recv,
    w_sem, a_zs, a_zr, a_ts, a_tr, a_ps, a_pr, b_ps, b_pr, b_ts, b_tr, b_zs, b_zr,
):
    ep, tp = lax.axis_index("ep"), lax.axis_index("tp")
    z, core = ep // CORES, ep % CORES
    other = 1 - core
    rows, width = tokens.shape
    half = n_z * rows
    units = gate_v.shape[1]
    tile = min(256, units)
    out_tile = min(256, width)

    def block(zz):
        return pl.ds(pl.multiple_of((core * n_z + zz) * rows, rows), rows)

    def core_rows(cc):
        return pl.ds(pl.multiple_of(cc * half, half), half)

    def features(tt):
        return pl.ds(pl.multiple_of(tt * width, width), width)

    weight_copies = []
    for kt in range(n_tp):
        part = features(flip(tp, kt))
        for side, (hbm, vmem) in enumerate(((w_gate, gate_v), (w_up, up_v))):
            copy = pltpu.make_async_copy(
                hbm.at[0, part, :], vmem.at[part, :], w_sem.at[2 * kt + side]
            )
            copy.start()
            weight_copies.append(copy)
    down_copy = pltpu.make_async_copy(w_down.at[0], down_v, w_sem.at[2 * n_tp])
    down_copy.start()

    barrier = pltpu.get_barrier_semaphore()
    peers = [(flip(z, k) * CORES + core, tp) for k in range(1, n_z)]
    peers += [(ep, flip(tp, k)) for k in range(1, n_tp)]
    peers += [(z * CORES + other, tp)]
    for peer in peers:
        pl.semaphore_signal(barrier, inc=1, device_id=peer, device_id_type=MESH)

    values = tokens[...].astype(jnp.float32)
    squares = jnp.sum(values * values, axis=1, keepdims=True)
    lane = lax.broadcasted_iota(jnp.int32, (rows, EXTRA), 1)
    place = lane % HALF_EXTRA
    side_values = jnp.where(place == SQUARES, squares, 0.0)
    for k in range(routes.shape[1]):
        side_values += jnp.where(place == routes[:, k : k + 1], route_weights[:, k : k + 1], 0.0)
    high = side_values.astype(jnp.bfloat16).astype(jnp.float32)
    side_values = jnp.where(lane < HALF_EXTRA, high, side_values - high)
    gathered[tp, block(z), :width] = (values * gain[...].astype(jnp.float32)).astype(jnp.bfloat16)
    gathered[tp, block(z), width:] = side_values.astype(jnp.bfloat16)
    pl.semaphore_wait(barrier, len(peers))

    def remote(src, dst, send, recv, peer):
        return pltpu.make_async_remote_copy(
            src_ref=src, dst_ref=dst, send_sem=send, recv_sem=recv,
            device_id=peer, device_id_type=MESH,
        )

    def z_peer(k):
        return (flip(z, k) * CORES + core, tp)

    def tp_peer(k):
        return (ep, flip(tp, k))

    partner = (z * CORES + other, tp)
    sent = []

    def send(*args):
        copy = remote(*args)
        copy.start()
        sent.append(copy)

    mine = gathered.at[tp, block(z), :]
    for kz in range(n_z - 1, 0, -1):
        send(mine, mine, a_zs.at[kz], a_zr.at[kz], z_peer(kz))
    for kz in range(n_z):
        here = gathered.at[tp, block(flip(z, kz)), :]
        if kz > 0:
            remote(here, here, a_zs.at[kz], a_zr.at[kz], z_peer(kz)).wait_recv()
        for kt in range(1, n_tp):
            send(here, here, a_ts.at[kt, kz], a_tr.at[kt, kz], tp_peer(kt))

    def to_partner(kt):
        if kt > 0:
            for kz in range(n_z):
                there = gathered.at[flip(tp, kt), block(flip(z, kz)), :]
                remote(there, there, a_ts.at[kt, kz], a_tr.at[kt, kz], tp_peer(kt)).wait_recv()
        ours = gathered.at[flip(tp, kt), core_rows(core), :]
        send(ours, ours, a_ps.at[kt], a_pr.at[kt], partner)

    to_partner(0)
    for kt in range(n_tp):
        if kt + 1 < n_tp:
            to_partner(kt + 1)
        source = flip(tp, kt)
        theirs = gathered.at[source, core_rows(other), :]
        remote(theirs, theirs, a_ps.at[kt], a_pr.at[kt], partner).wait_recv()
        weight_copies[2 * kt].wait()
        weight_copies[2 * kt + 1].wait()

        @pl.loop(0, units // tile)
        def _(n):
            columns = pl.ds(pl.multiple_of(n * tile, tile), tile)
            left = gathered[source, :, :width]
            for vmem, acc in ((gate_v, acc_gate), (up_v, acc_up)):
                product = jnp.dot(
                    left, vmem[features(source), columns], preferred_element_type=jnp.float32
                )
                if kt > 0:
                    product += acc[:, columns]
                acc[:, columns] = product

    lanes = lax.broadcasted_iota(jnp.int32, (half, EXTRA), 1)
    for at, cc in enumerate((other, core)):
        group = core_rows(cc)
        total = jnp.zeros((half, EXTRA), jnp.float32)
        for kt in range(n_tp):
            total += gathered[kt, group, width:].astype(jnp.float32)
        picked = jnp.where(lanes % HALF_EXTRA == SQUARES, total, 0.0)
        mean = jnp.sum(picked, axis=1, keepdims=True) / (n_tp * width)
        scale = lax.rsqrt(mean + 1e-05)
        chosen = jnp.where(
            lanes % HALF_EXTRA == ep, gathered[tp, group, width:].astype(jnp.float32), 0.0
        )
        weight = jnp.sum(chosen, axis=1, keepdims=True)
        gated = jnp.minimum(acc_gate[group, :] * scale, 7.0)
        upper = jnp.clip(acc_up[group, :] * scale, -7.0, 7.0)
        values = (upper + 1.0) * gated * jax.nn.sigmoid(1.702 * gated)
        hidden[at * half : (at + 1) * half, :] = (values * weight).astype(jnp.bfloat16)

    down_copy.wait()

    def pair_sum(kt):
        remote(
            pair_send.at[kt], pair_recv.at[kt], b_ps.at[kt], b_pr.at[kt], partner
        ).wait_recv()
        total = pair_own[kt] + pair_recv[kt].astype(jnp.float32)
        if kt == 0:
            pair_own[0] = total
        else:
            tp_send[kt] = total.astype(jnp.bfloat16)

    order = list(range(n_tp - 1, -1, -1))
    for step, kt in enumerate(order):
        target = flip(tp, kt)

        @pl.loop(0, width // out_tile)
        def _(n):
            columns = pl.ds(pl.multiple_of(n * out_tile, out_tile), out_tile)
            from_column = pl.multiple_of(target * width + n * out_tile, out_tile)
            product = jnp.dot(
                hidden[...], down_v[:, pl.ds(from_column, out_tile)],
                preferred_element_type=jnp.float32,
            )
            pair_send[kt, :, columns] = product[:half].astype(jnp.bfloat16)
            pair_own[kt, :, columns] = product[half:]

        send(pair_send.at[kt], pair_recv.at[kt], b_ps.at[kt], b_pr.at[kt], partner)
        if step > 0:
            pair_sum(order[step - 1])
        if step == n_tp - 1:
            break

    def z_rows(kz):
        return pl.ds(pl.multiple_of(flip(z, kz) * rows, rows), rows)

    def tp_copy(kt, kz):
        return remote(
            tp_send.at[kt, z_rows(kz), :], tp_recv.at[kt, z_rows(kz), :],
            b_ts.at[kt, kz], b_tr.at[kt, kz], tp_peer(kt),
        )

    for kz in range(n_z - 1, -1, -1):
        for kt in range(n_tp - 1, 0, -1):
            copy = tp_copy(kt, kz)
            copy.start()
            sent.append(copy)
    pair_sum(0)
    final = None
    for kz in range(n_z - 1, -1, -1):
        total = pair_own[0, z_rows(kz), :]
        for kt in range(n_tp - 1, 0, -1):
            tp_copy(kt, kz).wait_recv()
            total += tp_recv[kt, z_rows(kz), :].astype(jnp.float32)
        if kz > 0:
            z_send[kz] = total.astype(jnp.bfloat16)
            send(z_send.at[kz], z_recv.at[kz], b_zs.at[kz], b_zr.at[kz], z_peer(kz))
        else:
            final = total
    for kz in range(n_z - 1, 0, -1):
        remote(z_send.at[kz], z_recv.at[kz], b_zs.at[kz], b_zr.at[kz], z_peer(kz)).wait_recv()
        final += z_recv[kz].astype(jnp.float32)
    out[...] = final.astype(jnp.bfloat16)
    for copy in sent:
        copy.wait_send()


def shards(n_ep, n_tp, tokens, norm_gain, routes, route_weights, w_gate, w_up, w_down):
    rows, width = tokens.shape
    depth, units = w_gate.shape[1:]
    n_z = n_ep // CORES
    half = n_z * rows
    everyone = n_ep * rows
    bf16, f32, dma = jnp.bfloat16, jnp.float32, pltpu.SemaphoreType.DMA
    vmem = pl.BlockSpec(memory_space=pltpu.VMEM)
    anywhere = pl.BlockSpec(memory_space=pl.ANY)
    return pl.pallas_call(
        functools.partial(kernel, n_z, n_tp),
        out_shape=jax.ShapeDtypeStruct((rows, width), bf16),
        in_specs=[vmem] * 4 + [anywhere] * 3,
        out_specs=vmem,
        scratch_shapes=[
            pltpu.VMEM((depth, units), bf16),
            pltpu.VMEM((depth, units), bf16),
            pltpu.VMEM((units, depth), bf16),
            pltpu.VMEM((n_tp, everyone, width + EXTRA), bf16),
            pltpu.VMEM((everyone, units), f32),
            pltpu.VMEM((everyone, units), f32),
            pltpu.VMEM((everyone, units), bf16),
            pltpu.VMEM((n_tp, half, width), bf16),
            pltpu.VMEM((n_tp, half, width), bf16),
            pltpu.VMEM((n_tp, half, width), f32),
            pltpu.VMEM((n_tp, half, width), bf16),
            pltpu.VMEM((n_tp, half, width), bf16),
            pltpu.VMEM((n_z, rows, width), bf16),
            pltpu.VMEM((n_z, rows, width), bf16),
            dma((2 * n_tp + 1,)),
            dma((n_z,)), dma((n_z,)),
            dma((n_tp, n_z)), dma((n_tp, n_z)),
            dma((n_tp,)), dma((n_tp,)),
            dma((n_tp,)), dma((n_tp,)),
            dma((n_tp, n_z)), dma((n_tp, n_z)),
            dma((n_z,)), dma((n_z,)),
        ],
        compiler_params=pltpu.CompilerParams(
            collective_id=0, has_side_effects=True, vmem_limit_bytes=60 * 1024 * 1024
        ),
    )(tokens, norm_gain.reshape(1, -1), routes, route_weights, w_gate, w_up, w_down)


def solution(mesh):
    placed = (
        P("ep", "tp"),
        P("tp"),
        P("ep", None),
        P("ep", None),
        P("ep", None, "tp"),
        P("ep", None, "tp"),
        P("ep", "tp", None),
    )
    return jax.shard_map(
        functools.partial(shards, mesh.shape["ep"], mesh.shape["tp"]),
        mesh=mesh, in_specs=placed, out_specs=P("ep", "tp"), check_vma=False,
    )
```

time: 121 us -> 42.6 us (0.35)
  blocking collectives: 49.2 us -> 0 us
  Pallas kernels: 0 us -> 36.9 us
  waiting for transfers between devices: 35.7 us -> 0 us
  matrix products: 15.2 us -> 0 us
  between operations: 13.4 us -> 0.01 us
  starting transfers between devices: 4.62 us -> 0 us
  local copies, waits for them, and re-layouts: 1.03 us -> 5.35 us
    pallas_call x0 -> x1, Pallas kernels: none -> 36.9 us  [shards(): pl.pallas_call(functools.partial(kernel, n_z, n_tp), out_shape=jax.ShapeD...]
    all_to_all x1 -> x0, blocking collectives: 31.2 us -> none  [shards(): lax.all_to_all(outbound.reshape(groups, capacity, -1), 'ep', split_axis=0...]
    reduce_scatter x1 -> x0, waiting for transfers between devices: 26 us -> none  [shards(): lax.psum_scatter(partial_out, 'tp', scatter_dimension=1, tiled=True)]
    all_gather x2 -> x0, blocking collectives: 18 us -> none  [the longest x1 10.1 us: shards(): lax.all_gather(tokens, 'tp', axis=1, tiled=True)]
    dot_general x4 -> x0, matrix products: 15.2 us -> none  [the longest x1 9.29 us: shards(): jnp.dot(hidden, w_down[0], preferred_element_type=jnp.float32)]
    all_to_all x1 -> x0, waiting for transfers between devices: 9.62 us -> none  [shards(): lax.all_to_all(summed.reshape(groups, capacity, -1), 'ep', split_axis=0,...]
    all_to_all x1 -> x0, starting transfers between devices: 4.61 us -> none  [shards(): lax.all_to_all(summed.reshape(groups, capacity, -1), 'ep', split_axis=0,...]
    unnamed x3, local copies, waits for them, and re-layouts: 0.77 us -> 4.08 us
  transfers between devices with their start and end apart: 2 -> 0, of which waited for: 2 -> 0; matrix products, arithmetic and copies ran while one was open for 0% -> 0% of each run, Pallas kernels for 0% -> 0%
where the time goes in v1:
time: 42.6 us; the launch traced here: 42.3 us
  Pallas kernels  36.9 us (87%)
  local copies, waits for them, and re-layouts  5.35 us (13%)
    pallas_call x1, Pallas kernels, shards(): pl.pallas_call(functools.partial(kernel, n_z, n_tp), out_shape=jax.ShapeD...  36.9 us
    unnamed x3, local copies, waits for them, and re-layouts  4.08 us
    reshape x1, local copies, waits for them, and re-layouts, shards(): norm_gain.reshape(1, -1)  1.28 us

profile of v1, /device:TPU:0, one launch (start us, length us, event | category | flops | bytes accessed | tf_op | source)
XLA Modules:
  0.0 42.3 jit_solution(8733766040723034017)
XLA Ops:
  0.0 1.3 %reshape.3.gain = bf16[1,1024]{1,0:T(2,128)(2,1)} reshape(bf16[1024]{0:T(1024)(128)(2,1)} %param.8) | data formatting | bytes 4096 | tf_op jit(solution)/shard_map/reshape | solution.py:269
  1.3 1.4 %copy.8.routes = s32[16,4]{1,0:T(8,128)} copy(s32[16,4]{0,1:T(4,128)} %param.9) | data formatting | bytes 512 | tf_op args[2]
  2.6 1.3 %copy.9.route_weights = f32[16,4]{1,0:T(8,128)} copy(f32[16,4]{0,1:T(4,128)} %param.10) | data formatting | bytes 512 | tf_op args[3]
  4.0 36.9 %shard_map.73 = bf16[16,1024]{1,0:T(8,128)(2,1)} custom-call(bf16[16,1024]{1,0:T(8,128)(2,1)} %tokens.1, bf16[1,1024]{1,0:T(2,128)(2,1)} %reshape.3.gain, s32[16,4]{1,0:T(8,128)} %copy.8.routes, f32[16,4]{1,0:T(8,128)} %copy.9.route_weights, bf16[1,4096,1024]{2,1,0:T(8,128)(2,1)} %w_gate.1, bf16[1,4096,1024]{2,1,0:T(8,128)(2,1)} %w_up.1, ...), custom_call_target="tpu_custom_call" | custom-call | tf_op jit(solution)/shard_map/pallas_call | solution.py:238
  40.9 1.4 %copy.11 = bf16[16,1024]{1,0:T(8,128)(2,1)} copy(bf16[16,1024]{1,0:T(8,128)(2,1)} %shard_map.73) | data formatting | bytes 65536

commit v2 on v1

--- a/solution.py
+++ b/solution.py
@@ -25,11 +25,12 @@
 
 def kernel(
     n_z, n_tp,
-    tokens, gain, routes, route_weights, w_gate, w_up, w_down,
+    tokens_in, gain_in, routes_in, route_weights_in, w_gate, w_up, w_down,
     out,
+    tokens, gain, routes, route_weights,
     gate_v, up_v, down_v, gathered, acc_gate, acc_up, hidden,
     pair_send, pair_recv, pair_own, tp_send, tp_recv, z_send, z_recv,
-    w_sem, a_zs, a_zr, a_ts, a_tr, a_ps, a_pr, b_ps, b_pr, b_ts, b_tr, b_zs, b_zr,
+    in_sem, w_sem, a_zs, a_zr, a_ts, a_tr, a_ps, a_pr, b_ps, b_pr, b_ts, b_tr, b_zs, b_zr,
 ):
     ep, tp = lax.axis_index("ep"), lax.axis_index("tp")
     z, core = ep // CORES, ep % CORES
@@ -49,6 +50,22 @@
     def features(tt):
         return pl.ds(pl.multiple_of(tt * width, width), width)
 
+    barrier = pltpu.get_barrier_semaphore()
+    peers = [(flip(z, k) * CORES + core, tp) for k in range(1, n_z)]
+    peers += [(ep, flip(tp, k)) for k in range(1, n_tp)]
+    peers += [(z * CORES + other, tp)]
+    for peer in peers:
+        pl.semaphore_signal(barrier, inc=1, device_id=peer, device_id_type=MESH)
+
+    small = (
+        (tokens_in, tokens), (gain_in, gain), (routes_in, routes),
+        (route_weights_in, route_weights),
+    )
+    small_copies = [
+        pltpu.make_async_copy(src, dst, in_sem.at[i]) for i, (src, dst) in enumerate(small)
+    ]
+    for copy in small_copies:
+        copy.start()
     weight_copies = []
     for kt in range(n_tp):
         part = features(flip(tp, kt))
@@ -61,23 +78,25 @@
     down_copy = pltpu.make_async_copy(w_down.at[0], down_v, w_sem.at[2 * n_tp])
     down_copy.start()
 
-    barrier = pltpu.get_barrier_semaphore()
-    peers = [(flip(z, k) * CORES + core, tp) for k in range(1, n_z)]
-    peers += [(ep, flip(tp, k)) for k in range(1, n_tp)]
-    peers += [(z * CORES + other, tp)]
-    for peer in peers:
-        pl.semaphore_signal(barrier, inc=1, device_id=peer, device_id_type=MESH)
-
+    for copy in small_copies:
+        copy.wait()
     values = tokens[...].astype(jnp.float32)
     squares = jnp.sum(values * values, axis=1, keepdims=True)
     lane = lax.broadcasted_iota(jnp.int32, (rows, EXTRA), 1)
     place = lane % HALF_EXTRA
     side_values = jnp.where(place == SQUARES, squares, 0.0)
-    for k in range(routes.shape[1]):
-        side_values += jnp.where(place == routes[:, k : k + 1], route_weights[:, k : k + 1], 0.0)
+    diagonal = lax.broadcasted_iota(jnp.int32, (rows, rows), 0) == lax.broadcasted_iota(
+        jnp.int32, (rows, rows), 1
+    )
+    for k in range(routes.shape[0]):
+        expert = jnp.sum(jnp.where(diagonal, routes[k : k + 1, :], 0), axis=1, keepdims=True)
+        weight = jnp.sum(
+            jnp.where(diagonal, route_weights[k : k + 1, :], 0.0), axis=1, keepdims=True
+        )
+        side_values += jnp.where(place == expert, weight, 0.0)
     high = side_values.astype(jnp.bfloat16).astype(jnp.float32)
     side_values = jnp.where(lane < HALF_EXTRA, high, side_values - high)
-    gathered[tp, block(z), :width] = (values * gain[...].astype(jnp.float32)).astype(jnp.bfloat16)
+    gathered[tp, block(z), :width] = (values * gain[...].astype(jnp.float32).reshape(1, width)).astype(jnp.bfloat16)
     gathered[tp, block(z), width:] = side_values.astype(jnp.bfloat16)
     pl.semaphore_wait(barrier, len(peers))
 
@@ -120,9 +139,11 @@
         send(ours, ours, a_ps.at[kt], a_pr.at[kt], partner)
 
     to_partner(0)
+    passed = 1
     for kt in range(n_tp):
-        if kt + 1 < n_tp:
-            to_partner(kt + 1)
+        while passed < n_tp and passed <= (0, 2)[min(kt, 1)] + max(0, kt - 1):
+            to_partner(passed)
+            passed += 1
         source = flip(tp, kt)
         theirs = gathered.at[source, core_rows(other), :]
         remote(theirs, theirs, a_ps.at[kt], a_pr.at[kt], partner).wait_recv()
@@ -171,7 +192,22 @@
         else:
             tp_send[kt] = total.astype(jnp.bfloat16)
 
+    def z_rows(kz):
+        return pl.ds(pl.multiple_of(flip(z, kz) * rows, rows), rows)
+
+    def tp_copy(kt, kz):
+        return remote(
+            tp_send.at[kt, z_rows(kz), :], tp_recv.at[kt, z_rows(kz), :],
+            b_ts.at[kt, kz], b_tr.at[kt, kz], tp_peer(kt),
+        )
+
+    def send_sum(kt, kz):
+        copy = tp_copy(kt, kz)
+        copy.start()
+        sent.append(copy)
+
     order = list(range(n_tp - 1, -1, -1))
+    late = order[-3:-1]
     for step, kt in enumerate(order):
         target = flip(tp, kt)
 
@@ -188,24 +224,15 @@
 
         send(pair_send.at[kt], pair_recv.at[kt], b_ps.at[kt], b_pr.at[kt], partner)
         if step > 0:
-            pair_sum(order[step - 1])
-        if step == n_tp - 1:
-            break
-
-    def z_rows(kz):
-        return pl.ds(pl.multiple_of(flip(z, kz) * rows, rows), rows)
-
-    def tp_copy(kt, kz):
-        return remote(
-            tp_send.at[kt, z_rows(kz), :], tp_recv.at[kt, z_rows(kz), :],
-            b_ts.at[kt, kz], b_tr.at[kt, kz], tp_peer(kt),
-        )
+            done = order[step - 1]
+            pair_sum(done)
+            if done not in late:
+                for kz in range(n_z - 1, -1, -1):
+                    send_sum(done, kz)
 
     for kz in range(n_z - 1, -1, -1):
-        for kt in range(n_tp - 1, 0, -1):
-            copy = tp_copy(kt, kz)
-            copy.start()
-            sent.append(copy)
+        for kt in late:
+            send_sum(kt, kz)
     pair_sum(0)
     final = None
     for kz in range(n_z - 1, -1, -1):
@@ -237,10 +264,14 @@
     anywhere = pl.BlockSpec(memory_space=pl.ANY)
     return pl.pallas_call(
         functools.partial(kernel, n_z, n_tp),
-        out_shape=jax.ShapeDtypeStruct((rows, width), bf16),
-        in_specs=[vmem] * 4 + [anywhere] * 3,
+        out_shape=pltpu.VMEM((rows, width), bf16),
+        in_specs=[anywhere] * 7,
         out_specs=vmem,
         scratch_shapes=[
+            pltpu.VMEM((rows, width), bf16),
+            pltpu.VMEM((width,), bf16),
+            pltpu.VMEM(routes.T.shape, routes.dtype),
+            pltpu.VMEM(routes.T.shape, f32),
             pltpu.VMEM((depth, units), bf16),
             pltpu.VMEM((depth, units), bf16),
             pltpu.VMEM((units, depth), bf16),
@@ -255,6 +286,7 @@
             pltpu.VMEM((n_tp, half, width), bf16),
             pltpu.VMEM((n_z, rows, width), bf16),
             pltpu.VMEM((n_z, rows, width), bf16),
+            dma((4,)),
             dma((2 * n_tp + 1,)),
             dma((n_z,)), dma((n_z,)),
             dma((n_tp, n_z)), dma((n_tp, n_z)),
@@ -266,7 +298,7 @@
         compiler_params=pltpu.CompilerParams(
             collective_id=0, has_side_effects=True, vmem_limit_bytes=60 * 1024 * 1024
         ),
-    )(tokens, norm_gain.reshape(1, -1), routes, route_weights, w_gate, w_up, w_down)
+    )(tokens, norm_gain, routes.T, route_weights.T, w_gate, w_up, w_down)
 
 
 def solution(mesh):

time: 42.6 us -> 39.1 us (0.918)
  local copies, waits for them, and re-layouts: 5.35 us -> 0.62 us
  Pallas kernels: 36.9 us -> 38.3 us
    unnamed x3 -> x1, local copies, waits for them, and re-layouts: 4.08 us -> 0.62 us
    pallas_call x1, Pallas kernels: 36.9 us -> 38.3 us  [shards(): pl.pallas_call(functools.partial(kernel, n_z, n_tp), out_shape=pltpu.VMEM...]
    reshape x1 -> x0, local copies, waits for them, and re-layouts: 1.28 us -> none  [shards(): norm_gain.reshape(1, -1)]
where the time goes in v2:
time: 39.1 us; the launch traced here: 38.9 us
  Pallas kernels  38.3 us (98%)
  local copies, waits for them, and re-layouts  0.62 us (2%)
    pallas_call x1, Pallas kernels, shards(): pl.pallas_call(functools.partial(kernel, n_z, n_tp), out_shape=pltpu.VMEM...  38.3 us

profile of v2, /device:TPU:0, one launch (start us, length us, event | category | flops | bytes accessed | tf_op | source)
XLA Modules:
  0.0 38.9 jit_solution(4860370142486848007)
XLA Ops:
  0.0 38.3 %shard_map.73 = bf16[16,1024]{1,0:T(8,128)(2,1)S(1)} custom-call(bf16[16,1024]{1,0:T(8,128)(2,1)} %tokens_in.1, bf16[1024]{0:T(1024)(128)(2,1)} %gain_in.1, s32[4,16]{1,0:T(4,128)} %bitcast.2, f32[4,16]{1,0:T(4,128)} %bitcast.3, bf16[1,4096,1024]{2,1,0:T(8,128)(2,1)} %w_gate.1, bf16[1,4096,1024]{2,1,0:T(8,128)(2,1)} %w_up.1, bf16[1,1024,4096]{2,1,0:T(8,128)(2,1)} %w_down.1), custom_call_target="tpu_custom_call" | custom-call | tf_op jit(solution)/shard_map/pallas_call | solution.py:265
  38.3 0.6 %copy.9 = bf16[16,1024]{1,0:T(8,128)(2,1)} copy(bf16[16,1024]{1,0:T(8,128)(2,1)S(1)} %shard_map.73) | data formatting | bytes 65536
